TPU v7x, 32 devices: a whole 2x2x4 slice. The times are simulated.
32 devices in a mesh: dp: 4 (over y, x), kv: 4 (over z), tp: 2 (over core).
Axes of the slice: x: 2, y: 2, z: 4, core: 2. Of those that a mesh axis runs over, the one named last changes fastest.
Arguments:
- tokens: bfloat16 [256, 2048], P('dp', ('kv', 'tp')), parts along dimension 0, may hold values from -64 to 64, as said below
- lengths: int32 [32], P(('dp', 'kv', 'tp')), parts along dimension 0, may hold values from 1 to 8, 28 in all
- state: float32 [32, 16, 128, 128], P(('dp', 'kv', 'tp')), parts along dimension 0, may hold values from -1.8 to 1.8
- gain_first: float32 [2048], replicated, may hold values from 0.1 to 1.9
- first_gate: bfloat16 [2048, 5632], P(None, 'kv'), may hold values from -0.125 to 0.125
- first_up: bfloat16 [2048, 5632], P(None, 'kv'), may hold values from -0.125 to 0.125
- first_down: bfloat16 [5632, 2048], P('kv'), may hold values from -0.109375 to 0.109375
- gain_mix: float32 [2048], replicated, may hold values from 0.1 to 1.9
- query_weight: bfloat16 [2048, 2048], P(None, ('kv', 'tp')), may hold values from -0.125 to 0.125
- key_weight: bfloat16 [2048, 2048], P(None, ('kv', 'tp')), may hold values from -0.125 to 0.125
- value_weight: bfloat16 [2048, 2048], P(None, ('kv', 'tp')), may hold values from -0.125 to 0.125
- gating_weight: bfloat16 [2048, 2048], P(None, ('kv', 'tp')), may hold values from -0.125 to 0.125
- write_weight: bfloat16 [2048, 16], replicated, may hold values from -0.125 to 0.125
- forget_weight: bfloat16 [2048, 16], replicated, may hold values from -0.125 to 0.125
- forget_rate: float32 [16], replicated, may hold values from -4 to 1.5
- out_weight: bfloat16 [2048, 2048], P(None, ('kv', 'tp')), may hold values from -0.125 to 0.125
- gain_second: float32 [2048], replicated, may hold values from 0.1 to 1.9
- second_gate: bfloat16 [2048, 5632], P(None, 'kv'), may hold values from -0.125 to 0.125
- second_up: bfloat16 [2048, 5632], P(None, 'kv'), may hold values from -0.125 to 0.125
- second_down: bfloat16 [5632, 2048], P('kv'), may hold values from -0.109375 to 0.109375
Outputs:
- mixed_out: bfloat16 [256, 2048], P('dp', ('kv', 'tp')), parts along dimension 0
- new_state: float32 [32, 16, 128, 128], P(('dp', 'kv', 'tp')), parts along dimension 0
There are 4 independent parts, one for each index of `dp`. A program takes and returns all parts, laid end to end along the dimension named above; an argument that names none is the same for every part. Nothing has to cross between parts.
Inputs may be any that keep to these rules, and one draw needn't show every extreme that they name: Activations of the new tokens. `lengths`: the live new tokens of each sequence; within each independent group of 8 sequences (one part along dp) they sum to seven halves of 8, rounded down, and some sequence of each group has all 8 live.
All inputs are finite; a program needn't handle non-finite values.
Results may differ from a plain program's by a relative error of at most 0.0058.
Values may be sent and summed in bfloat16 or wider, within the bound.
A program may use at most 128 MiB of HBM per device.

v0:
```python
import math
import jax
import jax.numpy as jnp
from jax import lax
from jax.sharding import PartitionSpec as P

HEADS = 16
HEAD = 128
BLK = 8
EPSILON = 1e-06


def fold_step(gain, gate_cols, up_cols, portion):
    values = portion.astype(jnp.float32)
    scaled = (values * gain).astype(jnp.bfloat16)
    gate_acc = jnp.dot(scaled, gate_cols, preferred_element_type=jnp.float32)
    up_acc = jnp.dot(scaled, up_cols, preferred_element_type=jnp.float32)
    squares = jnp.sum(values * values, axis=1)
    return (gate_acc, up_acc, squares)


def finish_units(gate_acc, up_acc, squares, channels, down_rows):
    row_scale = lax.rsqrt(squares / channels + EPSILON)[:, None]
    hidden = (jax.nn.silu(gate_acc * row_scale) * (up_acc * row_scale)).astype(jnp.bfloat16)
    return jnp.dot(hidden, down_rows, preferred_element_type=jnp.float32)


def feed_forward(hidden_in, gain, w_gate, w_up, w_down):
    channels = gain.shape[0]
    paired = lax.all_to_all(hidden_in, "tp", split_axis=0, concat_axis=1, tiled=True)
    gate_acc, up_acc, squares = fold_step(
        gain, w_gate, w_up, lax.all_gather(paired, "kv", axis=1, tiled=True)
    )
    ffn_term = finish_units(gate_acc, up_acc, squares, channels, w_down)
    partial_value = lax.psum_scatter(ffn_term, "kv", scatter_dimension=1, tiled=True)
    summed = lax.all_to_all(partial_value, "tp", split_axis=1, concat_axis=0, tiled=True)
    return (hidden_in.astype(jnp.float32) + 0.5 * summed).astype(jnp.bfloat16)


def delta_block(query, key_in, value, gating, write_pre, forget_pre, rates, live, state):
    seq_count, block_len, head_count, head_size = query.shape
    precise = lax.Precision.HIGHEST
    query_unit = (
        query
        * lax.rsqrt(jnp.sum(query * query, axis=-1, keepdims=True) + EPSILON)
        / math.sqrt(head_size)
    )
    key_unit = key_in * lax.rsqrt(jnp.sum(key_in * key_in, axis=-1, keepdims=True) + EPSILON)
    live_rows = live[:, :, None]
    write_gate = jax.nn.sigmoid(write_pre) * live_rows
    forget = -jnp.exp(rates)[None, None, :] * jax.nn.softplus(forget_pre) * live_rows
    cumulative = jnp.cumsum(forget, axis=1)
    cum_heads = jnp.transpose(cumulative, (0, 2, 1))
    positions = jnp.arange(block_len)
    causal = positions[:, None] >= positions[None, :]
    strict = positions[:, None] > positions[None, :]
    differ = jnp.minimum(cum_heads[:, :, :, None] - cum_heads[:, :, None, :], 0.0)
    decay_mat = jnp.where(causal, jnp.exp(differ), 0.0)
    key_dots = jnp.einsum("sthd,suhd->shtu", key_unit, key_unit, precision=precise)
    write_heads = jnp.transpose(write_gate, (0, 2, 1))
    strict_part = jnp.where(strict, write_heads[:, :, :, None] * decay_mat * key_dots, 0.0)
    identity = jnp.eye(block_len, dtype=jnp.float32)
    squared = jnp.einsum("shtu,shuv->shtv", strict_part, strict_part, precision=precise)
    fourth = jnp.einsum("shtu,shuv->shtv", squared, squared, precision=precise)
    inverse = jnp.einsum(
        "shtu,shuv->shtv", identity - strict_part, identity + squared, precision=precise
    )
    inverse = jnp.einsum("shtu,shuv->shtv", inverse, identity + fourth, precision=precise)
    growth = jnp.exp(cumulative)
    target = jnp.einsum(
        "shtu,suhv->sthv", inverse, write_gate[..., None] * value, precision=precise
    )
    key_mix = jnp.einsum(
        "shtu,suhk->sthk", inverse, (write_gate * growth)[..., None] * key_unit, precision=precise
    )
    update = target - jnp.einsum("sthk,shkv->sthv", key_mix, state, precision=precise)
    scores = jnp.einsum("sthd,suhd->shtu", query_unit, key_unit, precision=precise) * decay_mat
    attend = jnp.einsum("sthk,shkv->sthv", query_unit * growth[..., None], state, precision=precise)
    attend = attend + jnp.einsum("shtu,suhv->sthv", scores, update, precision=precise)
    final_cum = cumulative[:, -1:, :]
    fading = jnp.exp(final_cum - cumulative)
    new_state = jnp.exp(final_cum[:, 0, :])[:, :, None, None] * state
    new_state = new_state + jnp.einsum(
        "sthk,sthv->shkv", key_unit * fading[..., None], update, precision=precise
    )
    normed = attend * lax.rsqrt(jnp.mean(attend * attend, axis=-1, keepdims=True) + EPSILON)
    normed = normed * jax.nn.silu(gating) * live[:, :, None, None]
    mixed_heads = normed.reshape(seq_count * block_len, head_count * head_size).astype(jnp.bfloat16)
    return (mixed_heads, new_state)


def per_device(
    tokens,
    lengths,
    state,
    gain_first,
    first_gate,
    first_up,
    first_down,
    gain_mix,
    query_weight,
    key_weight,
    value_weight,
    gating_weight,
    write_weight,
    forget_weight,
    forget_rate,
    out_weight,
    gain_second,
    second_gate,
    second_up,
    second_down,
):
    after_first = feed_forward(tokens, gain_first, first_gate, first_up, first_down)
    seq_count = lengths.shape[0]
    own_count = seq_count * BLK
    whole_rows = lax.all_gather(after_first, ("kv", "tp"), axis=1, tiled=True)
    scaled_all = (whole_rows.astype(jnp.float32) * gain_mix).astype(jnp.bfloat16)
    stacked = jnp.stack(
        [
            jnp.dot(scaled_all, matrix, preferred_element_type=jnp.float32)
            for matrix in (query_weight, key_weight, value_weight, gating_weight)
        ]
    )
    owned = lax.all_to_all(
        stacked.astype(jnp.bfloat16), ("kv", "tp"), split_axis=1, concat_axis=2, tiled=True
    ).astype(stacked.dtype)
    row_start = lax.axis_index(("kv", "tp")) * own_count
    own_values = lax.dynamic_slice_in_dim(whole_rows, row_start, own_count, 0).astype(jnp.float32)
    own_scaled = lax.dynamic_slice_in_dim(scaled_all, row_start, own_count, 0)
    mix_scale = lax.rsqrt(jnp.mean(own_values * own_values, axis=1, keepdims=True) + EPSILON)
    query = (owned[0] * mix_scale).reshape(seq_count, BLK, HEADS, HEAD)
    key_in = (owned[1] * mix_scale).reshape(seq_count, BLK, HEADS, HEAD)
    value = (owned[2] * mix_scale).reshape(seq_count, BLK, HEADS, HEAD)
    gating = (owned[3] * mix_scale).reshape(seq_count, BLK, HEADS, HEAD)
    write_pre = (
        jnp.dot(own_scaled, write_weight, preferred_element_type=jnp.float32) * mix_scale
    ).reshape(seq_count, BLK, HEADS)
    forget_pre = (
        jnp.dot(own_scaled, forget_weight, preferred_element_type=jnp.float32) * mix_scale
    ).reshape(seq_count, BLK, HEADS)
    positions = jnp.arange(BLK, dtype=jnp.int32)
    live = (positions[None, :] < lengths[:, None]).astype(jnp.float32)
    mixed_heads, new_state = delta_block(
        query, key_in, value, gating, write_pre, forget_pre, forget_rate, live, state
    )
    half_cols = mixed_heads.shape[1] // 2
    portion = lax.all_gather(mixed_heads, ("kv", "tp"), axis=0, tiled=True)
    first_half = jnp.dot(
        portion[:, :half_cols], out_weight[:half_cols], preferred_element_type=jnp.float32
    ).astype(jnp.bfloat16)
    second_half = jnp.dot(
        portion[:, half_cols:], out_weight[half_cols:], preferred_element_type=jnp.float32
    ).astype(jnp.bfloat16)
    first_half, second_half = lax.optimization_barrier((first_half, second_half))
    mixed_sum = first_half.astype(jnp.float32) + second_half.astype(jnp.float32)
    after_mix = (after_first.astype(jnp.float32) + mixed_sum).astype(jnp.bfloat16)
    mixed_out = feed_forward(after_mix, gain_second, second_gate, second_up, second_down)
    return (mixed_out, new_state)


def solution(mesh):
    in_specs = (
        P("dp", ("kv", "tp")),
        P(("dp", "kv", "tp")),
        P(("dp", "kv", "tp"), None, None, None),
        P(),
        P(None, "kv"),
        P(None, "kv"),
        P("kv", None),
        P(),
        P(None, ("kv", "tp")),
        P(None, ("kv", "tp")),
        P(None, ("kv", "tp")),
        P(None, ("kv", "tp")),
        P(),
        P(),
        P(),
        P(None, ("kv", "tp")),
        P(),
        P(None, "kv"),
        P(None, "kv"),
        P("kv", None),
    )
    out_specs = (P("dp", ("kv", "tp")), P(("dp", "kv", "tp"), None, None, None))
    return jax.shard_map(
        per_device, mesh=mesh, in_specs=in_specs, out_specs=out_specs, check_vma=False
    )
```

profile of v0, /device:TPU:0, one launch (start us, length us, event | category | flops | bytes accessed | tf_op | source)
XLA Modules:
  0.0 174.8 jit_solution(16179178874863830319)
XLA Ops:
  7.2 4.8 %all_to_all.73 = bf16[2,32,256]{2,1,0:T(8,128)(2,1)S(1)} all-to-all(bf16[2,32,256]{2,1,0:T(8,128)(2,1)} %bitcast.150), channel_id=1, replica_groups=mesh['dp'=4,'kv'=4,'tp'=2] {'tp'}, dimensions={0} | all-to-all | bytes 65536 | tf_op jit(solution)/shard_map/all_to_all | solution.py:30
  12.0 15.1 %all_gather.12 = bf16[32,2048]{1,0:T(8,128)(2,1)S(1)} all-gather(bf16[32,512]{1,0:T(8,128)(2,1)S(1)} %bitcast.146), channel_id=1, replica_groups=mesh['dp'=4,'kv'=4,'tp'=2] {'kv'}, dimensions={1}, use_global_device_ids=true | all-gather | bytes 163840 | tf_op jit(solution)/shard_map/all_gather | solution.py:32
  27.2 3.7 %convolution_multiply_fusion.3 = f32[32,1408]{1,0:T(8,128)S(1)} fusion(bf16[2048,1408]{1,0:T(8,128)(2,1)} %param.24, bf16[32,2048]{1,0:T(8,128)(2,1)S(1)} %all_gather.12, f32[2048]{0:T(1024)} %param.23, f32[32]{0:T(128)S(1)} %add_rsqrt_fusion.5), kind=kOutput, calls=%fused_computation.5 | convolution fusion | flops 184791040 | bytes 6086784 | tf_op jit(solution)/shard_map/dot_general | solution.py:16
  31.0 7.1 %fusion.21 = f32[32,2048]{1,0:T(8,128)} fusion(bf16[1408,2048]{1,0:T(8,128)(2,1)} %param.26, bf16[2048,1408]{1,0:T(8,128)(2,1)} %param.25, f32[32,1408]{1,0:T(8,128)S(1)} %convolution_multiply_fusion.3, bf16[32,2048]{1,0:T(8,128)(2,1)S(1)} %all_gather.12, f32[2048]{0:T(1024)S(1)} %copy-done.4, f32[32]{0:T(128)S(1)} %add_rsqrt_fusion.5), kind=kOutput, calls=%fused_computation.41 | convolution fusion | flops 369610752 | bytes 12116096 | tf_op jit(solution)/shard_map/dot_general | solution.py:25
  38.9 20.5 %reduce-scatter.3.cloned.1.call-done = f32[32,512]{1,0:T(8,128)} async-done(((f32[32,2048]{1,0:T(8,128)}), f32[32,512]{1,0:T(8,128)}) %reduce-scatter.3.cloned.1.call-update) | async-done | bytes 65552 | tf_op jit(solution)/shard_map/reduce_scatter | solution.py:35
  60.2 3.8 %all_to_all.74 = f32[32,2,256]{2,0,1:T(8,128)S(1)} all-to-all(f32[32,2,256]{2,0,1:T(8,128)S(1)} %bitcast.144), channel_id=1, replica_groups=mesh['dp'=4,'kv'=4,'tp'=2] {'tp'}, dimensions={1} | all-to-all | bytes 131072 | tf_op jit(solution)/shard_map/all_to_all | solution.py:36
  64.0 14.3 %all_gather.13 = bf16[64,2048]{1,0:T(8,128)(2,1)S(1)} all-gather(bf16[64,256]{1,0:T(8,128)(2,1)S(1)} %fusion.51), channel_id=1, replica_groups=mesh['dp'=4,'kv'=4,'tp'=2] {'kv','tp'}, dimensions={1}, use_global_device_ids=true | all-gather | bytes 294912 | tf_op jit(solution)/shard_map/all_gather | solution.py:117
  79.2 1.5 fusion.10
  80.7 1.5 fusion.9
  83.0 3.4 %all-to-all-start.2 = ((bf16[4,64,256]{2,0,1:T(4,128)(2,1)}), bf16[4,64,256]{2,0,1:T(4,128)(2,1)S(1)}, u32[]{:S(2)}, u32[]{:S(2)}) async-start(bf16[4,64,256]{2,0,1:T(4,128)(2,1)} %copy.99), calls=%async_computation.3 | async-start | bytes 262144 | tf_op jit(solution)/shard_map/all_to_all | solution.py:125
  86.7 0.9 fusion.80
  87.8 5.3 %all-to-all-done.2 = bf16[4,64,256]{2,0,1:T(4,128)(2,1)S(1)} async-done(((bf16[4,64,256]{2,0,1:T(4,128)(2,1)}), bf16[4,64,256]{2,0,1:T(4,128)(2,1)S(1)}, u32[]{:S(2)}, u32[]{:S(2)}) %all-to-all-start.2) | async-done | bytes 131104 | tf_op jit(solution)/shard_map/all_to_all | solution.py:125
  96.0 1.0 convolution_bitcast_fusion.3
  96.9 1.0 fusion.7
  98.5 14.2 %all_gather.14 = bf16[64,2048]{1,0:T(8,128)(2,1)S(1)} all-gather(bf16[8,2048]{1,0:T(8,128)(2,1)S(1)} %fusion.70), channel_id=1, replica_groups=mesh['dp'=4,'kv'=4,'tp'=2] {'kv','tp'}, dimensions={0}, use_global_device_ids=true | all-gather | bytes 294912 | tf_op jit(solution)/shard_map/all_gather | solution.py:148
  112.8 1.2 convolution_convert_fusion
  114.0 1.2 convolution_convert_fusion.1
  115.3 3.7 %all_to_all.75 = bf16[2,32,256]{2,1,0:T(8,128)(2,1)S(1)} all-to-all(bf16[2,32,256]{2,1,0:T(8,128)(2,1)S(1)} %bitcast.143), channel_id=1, replica_groups=mesh['dp'=4,'kv'=4,'tp'=2] {'tp'}, dimensions={0} | all-to-all | bytes 65536 | tf_op jit(solution)/shard_map/all_to_all | solution.py:30
  119.0 13.6 %all_gather.15 = bf16[32,2048]{1,0:T(8,128)(2,1)S(1)} all-gather(bf16[32,512]{1,0:T(8,128)(2,1)S(1)} %bitcast.147), channel_id=1, replica_groups=mesh['dp'=4,'kv'=4,'tp'=2] {'kv'}, dimensions={1}, use_global_device_ids=true | all-gather | bytes 163840 | tf_op jit(solution)/shard_map/all_gather | solution.py:32
  132.7 3.6 %convolution_multiply_fusion.1 = f32[32,1408]{1,0:T(8,128)S(1)} fusion(bf16[2048,1408]{1,0:T(8,128)(2,1)} %param.37, bf16[32,2048]{1,0:T(8,128)(2,1)S(1)} %all_gather.15, f32[2048]{0:T(1024)S(1)} %copy-done.5, f32[32]{0:T(128)S(1)} %add_rsqrt_fusion.3), kind=kOutput, calls=%fused_computation.2 | convolution fusion | flops 184791040 | bytes 6086784 | tf_op jit(solution)/shard_map/dot_general | solution.py:16
  136.4 7.0 %fusion.20 = f32[32,2048]{1,0:T(8,128)} fusion(bf16[1408,2048]{1,0:T(8,128)(2,1)} %param.39, bf16[2048,1408]{1,0:T(8,128)(2,1)} %param.38, f32[32,1408]{1,0:T(8,128)S(1)} %convolution_multiply_fusion.1, bf16[32,2048]{1,0:T(8,128)(2,1)S(1)} %all_gather.15, f32[2048]{0:T(1024)S(1)} %copy-done.5, f32[32]{0:T(128)S(1)} %add_rsqrt_fusion.3), kind=kOutput, calls=%fused_computation.40 | convolution fusion | flops 369610752 | bytes 12116096 | tf_op jit(solution)/shard_map/dot_general | solution.py:25
  143.5 2.8 %fusion.4 = f32[1,16,128,128]{3,2,1,0:T(8,128)} fusion(f32[8,16,128]{2,0,1:T(8,128)S(1)} %fusion.7, f32[1,16,128,128]{3,2,1,0:T(8,128)S(1)} %copy-done.1, f32[16]{0:T(128)S(1)} %fusion.86, f32[8,16,128]{2,1,0:T(8,128)S(1)} %get-tuple-element.20), kind=kOutput, calls=%fused_computation.9 | convolution fusion | flops 25690112 | bytes 2228288 | tf_op jit(solution)/shard_map/sthk,sthv->shkv/dot_general | solution.py:83
  146.3 16.4 %reduce-scatter.5.cloned.1.call-done = f32[32,512]{1,0:T(8,128)} async-done(((f32[32,2048]{1,0:T(8,128)}), f32[32,512]{1,0:T(8,128)}) %reduce-scatter.5.cloned.1.call-update) | async-done | bytes 65552 | tf_op jit(solution)/shard_map/reduce_scatter | solution.py:35
  163.6 3.8 %all_to_all.76 = f32[32,2,256]{2,0,1:T(8,128)S(1)} all-to-all(f32[32,2,256]{2,0,1:T(8,128)S(1)} %bitcast.145), channel_id=1, replica_groups=mesh['dp'=4,'kv'=4,'tp'=2] {'tp'}, dimensions={1} | all-to-all | bytes 131072 | tf_op jit(solution)/shard_map/all_to_all | solution.py:36
  (79 shorter events, 8.1 us)
Async XLA Ops:
  7.2 71.4 %copy-start = (bf16[2048,256]{1,0:T(8,128)(2,1)S(1)}, bf16[2048,256]{1,0:T(8,128)(2,1)}, u32[]{:S(2)}) copy-start(bf16[2048,256]{1,0:T(8,128)(2,1)} %param.31) | copy-start | bytes 3145732
  7.2 23.7 %copy-start.4 = (f32[2048]{0:T(1024)S(1)}, f32[2048]{0:T(1024)}, u32[]{:S(2)}) copy-start(f32[2048]{0:T(1024)} %param.23) | copy-start | bytes 24580
  7.2 52.2 %reduce-scatter.3.cloned.1.call-start = ((), (), s32[]{:S(2)}) async-start(), calls=%async_computation.7 | async-start | bytes 327680 | tf_op jit(solution)/shard_map/reduce_scatter | solution.py:35
  30.9 7.9 %copy-start.8 = (f32[16]{0:T(128)S(1)}, f32[16]{0:T(128)}, u32[]{:S(2)}) copy-start(f32[16]{0:T(128)} %param.34) | copy-start | bytes 196
  30.9 33.1 %copy-start.3 = (bf16[64,256]{1,0:T(8,128)(2,1)S(1)}, bf16[64,256]{1,0:T(8,128)(2,1)}, u32[]{:S(2)}) copy-start(bf16[64,256]{1,0:T(8,128)(2,1)} %param.20) | copy-start | bytes 98308
  30.9 47.6 %copy-start.6 = (f32[2048]{0:T(1024)S(1)}, f32[2048]{0:T(1024)}, u32[]{:S(2)}) copy-start(f32[2048]{0:T(1024)} %param.27) | copy-start | bytes 24580
  30.9 47.9 %copy-start.2 = (bf16[2048,256]{1,0:T(8,128)(2,1)S(1)}, bf16[2048,256]{1,0:T(8,128)(2,1)}, u32[]{:S(2)}) copy-start(bf16[2048,256]{1,0:T(8,128)(2,1)} %param.30) | copy-start | bytes 3145732
  38.1 48.4 %copy-start.7 = (bf16[2048,16]{0,1:T(8,128)(2,1)S(1)}, bf16[2048,16]{0,1:T(8,128)(2,1)}, u32[]{:S(2)}) copy-start(bf16[2048,16]{0,1:T(8,128)(2,1)} %param.33) | copy-start | bytes 196612
  64.0 31.9 %copy-start.1 = (f32[1,16,128,128]{3,2,1,0:T(8,128)S(1)}, f32[1,16,128,128]{3,2,1,0:T(8,128)}, u32[]{:S(2)}) copy-start(f32[1,16,128,128]{3,2,1,0:T(8,128)} %param.22) | copy-start | bytes 3145732
  80.7 52.0 %copy-start.5 = (f32[2048]{0:T(1024)S(1)}, f32[2048]{0:T(1024)}, u32[]{:S(2)}) copy-start(f32[2048]{0:T(1024)} %param.36) | copy-start | bytes 24580
  83.0 10.1 %all-to-all-start.2 = ((bf16[4,64,256]{2,0,1:T(4,128)(2,1)}), bf16[4,64,256]{2,0,1:T(4,128)(2,1)S(1)}, u32[]{:S(2)}, u32[]{:S(2)}) async-start(bf16[4,64,256]{2,0,1:T(4,128)(2,1)} %copy.99), calls=%async_computation.3 | async-start | bytes 262144 | tf_op jit(solution)/shard_map/all_to_all | solution.py:125
  86.4 76.3 %reduce-scatter.5.cloned.1.call-start = ((), (), s32[]{:S(2)}) async-start(), calls=%async_computation.8 | async-start | bytes 327680 | tf_op jit(solution)/shard_map/reduce_scatter | solution.py:35
Sparse Core Ops, SparseCore 0:
  38.2 21.0 reduce-scatter.2
  143.6 19.1 reduce-scatter.4
where the time goes:
time: 176 us; the launch traced here: 175 us
  blocking collectives  73.2 us (42%)
  waiting for transfers between devices  42.3 us (24%)
  matrix products  35.8 us (20%)
  between operations  15.2 us (9%)
  starting transfers between devices  3.45 us (2%)
  local copies, waits for them, and re-layouts  3.13 us (2%)
  other arithmetic  1.76 us (1%)
    reduce_scatter x2, waiting for transfers between devices, feed_forward(): lax.psum_scatter(ffn_term, 'kv', scatter_dimension=1, tiled=True)  36.9 us
    all_gather x2, blocking collectives, feed_forward(): lax.all_gather(paired, 'kv', axis=1, tiled=True)  28.6 us
    all_gather x1, blocking collectives, per_device(): whole_rows = lax.all_gather(after_first, ('kv', 'tp'), axis=1, tiled=True)  14.3 us
    all_gather x1, blocking collectives, per_device(): portion = lax.all_gather(mixed_heads, ('kv', 'tp'), axis=0, tiled=True)  14.2 us
    dot_general x2, matrix products, finish_units(): return jnp.dot(hidden, down_rows, preferred_element_type=jnp.float32)  14.2 us
    all_to_all x2, blocking collectives, feed_forward(): lax.all_to_all(hidden_in, 'tp', split_axis=0, concat_axis=1, tiled=True)  8.52 us
    all_to_all x2, blocking collectives, feed_forward(): lax.all_to_all(partial_value, 'tp', split_axis=1, concat_axis=0, tiled=True)  7.56 us
    dot_general x2, matrix products, fold_step(): gate_acc = jnp.dot(scaled, gate_cols, preferred_element_type=jnp.float32)  7.31 us
  transfers between devices with their start and end apart: 3, of which 3 were waited for; matrix products, arithmetic and copies ran while one was open for 2% of the time, Pallas kernels for 0%

commit v1 on v0

--- a/solution.py
+++ b/solution.py
@@ -33,7 +33,12 @@
     )
     ffn_term = finish_units(gate_acc, up_acc, squares, channels, w_down)
     partial_value = lax.psum_scatter(ffn_term, "kv", scatter_dimension=1, tiled=True)
-    summed = lax.all_to_all(partial_value, "tp", split_axis=1, concat_axis=0, tiled=True)
+    summed = jnp.concatenate(
+        lax.all_to_all(
+            jnp.stack(jnp.split(partial_value, lax.axis_size("tp"), axis=1)), "tp", 0, 0
+        ),
+        axis=0,
+    )
     return (hidden_in.astype(jnp.float32) + 0.5 * summed).astype(jnp.bfloat16)
 
 

time: 176 us -> 176 us (level)
  no operation moved by 1% of the time
where the time goes in v1:
time: 176 us; the launch traced here: 175 us
  blocking collectives  73.3 us (42%)
  waiting for transfers between devices  42.2 us (24%)
  matrix products  35.8 us (20%)
  between operations  15.2 us (9%)
  starting transfers between devices  3.45 us (2%)
  local copies, waits for them, and re-layouts  3 us (2%)
  other arithmetic  1.77 us (1%)
    reduce_scatter x2, waiting for transfers between devices, feed_forward(): lax.psum_scatter(ffn_term, 'kv', scatter_dimension=1, tiled=True)  36.9 us
    all_gather x2, blocking collectives, feed_forward(): lax.all_gather(paired, 'kv', axis=1, tiled=True)  28.6 us
    all_gather x1, blocking collectives, per_device(): whole_rows = lax.all_gather(after_first, ('kv', 'tp'), axis=1, tiled=True)  14.3 us
    all_gather x1, blocking collectives, per_device(): portion = lax.all_gather(mixed_heads, ('kv', 'tp'), axis=0, tiled=True)  14.2 us
    dot_general x2, matrix products, finish_units(): return jnp.dot(hidden, down_rows, preferred_element_type=jnp.float32)  14.2 us
    all_to_all x2, blocking collectives, feed_forward(): lax.all_to_all(hidden_in, 'tp', split_axis=0, concat_axis=1, tiled=True)  8.52 us
    all_to_all x2, blocking collectives, feed_forward(): lax.all_to_all(jnp.stack(jnp.split(partial_value, lax.axis_size('tp'), ax...  7.58 us
    dot_general x2, matrix products, fold_step(): gate_acc = jnp.dot(scaled, gate_cols, preferred_element_type=jnp.float32)  7.31 us
  transfers between devices with their start and end apart: 3, of which 3 were waited for; matrix products, arithmetic and copies ran while one was open for 2% of the time, Pallas kernels for 0%

profile of v1, /device:TPU:0, one launch (start us, length us, event | category | flops | bytes accessed | tf_op | source)
XLA Modules:
  0.0 174.7 jit_solution(2432774181499316795)
XLA Ops:
  7.2 4.8 %all_to_all.57 = bf16[2,32,256]{2,1,0:T(8,128)(2,1)S(1)} all-to-all(bf16[2,32,256]{2,1,0:T(8,128)(2,1)} %bitcast.144), channel_id=1, replica_groups=mesh['dp'=4,'kv'=4,'tp'=2] {'tp'}, dimensions={0} | all-to-all | bytes 65536 | tf_op jit(solution)/shard_map/all_to_all | solution.py:30
  12.0 15.1 %all_gather.12 = bf16[32,2048]{1,0:T(8,128)(2,1)S(1)} all-gather(bf16[32,512]{1,0:T(8,128)(2,1)S(1)} %bitcast.140), channel_id=1, replica_groups=mesh['dp'=4,'kv'=4,'tp'=2] {'kv'}, dimensions={1}, use_global_device_ids=true | all-gather | bytes 163840 | tf_op jit(solution)/shard_map/all_gather | solution.py:32
  27.2 3.7 %convolution_multiply_fusion.3 = f32[32,1408]{1,0:T(8,128)S(1)} fusion(bf16[2048,1408]{1,0:T(8,128)(2,1)} %param.24, bf16[32,2048]{1,0:T(8,128)(2,1)S(1)} %all_gather.12, f32[2048]{0:T(1024)} %param.23, f32[32]{0:T(128)S(1)} %add_rsqrt_fusion.5), kind=kOutput, calls=%fused_computation.5 | convolution fusion | flops 184791040 | bytes 6086784 | tf_op jit(solution)/shard_map/dot_general | solution.py:16
  31.0 7.1 %fusion.21 = f32[32,2048]{1,0:T(8,128)} fusion(bf16[1408,2048]{1,0:T(8,128)(2,1)} %param.26, bf16[2048,1408]{1,0:T(8,128)(2,1)} %param.25, f32[32,1408]{1,0:T(8,128)S(1)} %convolution_multiply_fusion.3, bf16[32,2048]{1,0:T(8,128)(2,1)S(1)} %all_gather.12, f32[2048]{0:T(1024)S(1)} %copy-done.4, f32[32]{0:T(128)S(1)} %add_rsqrt_fusion.5), kind=kOutput, calls=%fused_computation.41 | convolution fusion | flops 369610752 | bytes 12116096 | tf_op jit(solution)/shard_map/dot_general | solution.py:25
  38.9 20.5 %reduce-scatter.3.cloned.1.call-done = f32[32,512]{1,0:T(8,128)} async-done(((f32[32,2048]{1,0:T(8,128)}), f32[32,512]{1,0:T(8,128)}) %reduce-scatter.3.cloned.1.call-update) | async-done | bytes 65552 | tf_op jit(solution)/shard_map/reduce_scatter | solution.py:35
  60.2 3.8 %all_to_all.58 = f32[2,32,256]{2,1,0:T(8,128)S(1)} all-to-all(f32[2,32,256]{2,1,0:T(8,128)S(1)} %pad_maximum_fusion.1), channel_id=1, replica_groups=mesh['dp'=4,'kv'=4,'tp'=2] {'tp'}, dimensions={0} | all-to-all | bytes 131072 | tf_op jit(solution)/shard_map/all_to_all | solution.py:37
  64.0 14.3 %all_gather.13 = bf16[64,2048]{1,0:T(8,128)(2,1)S(1)} all-gather(bf16[64,256]{1,0:T(8,128)(2,1)S(1)} %fusion.51), channel_id=1, replica_groups=mesh['dp'=4,'kv'=4,'tp'=2] {'kv','tp'}, dimensions={1}, use_global_device_ids=true | all-gather | bytes 294912 | tf_op jit(solution)/shard_map/all_gather | solution.py:122
  79.1 1.5 fusion.10
  80.7 1.5 fusion.9
  83.0 3.4 %all-to-all-start.2 = ((bf16[4,64,256]{2,0,1:T(4,128)(2,1)}), bf16[4,64,256]{2,0,1:T(4,128)(2,1)S(1)}, u32[]{:S(2)}, u32[]{:S(2)}) async-start(bf16[4,64,256]{2,0,1:T(4,128)(2,1)} %copy.88), calls=%async_computation.3 | async-start | bytes 262144 | tf_op jit(solution)/shard_map/all_to_all | solution.py:130
  86.7 0.9 fusion.80
  87.8 5.3 %all-to-all-done.2 = bf16[4,64,256]{2,0,1:T(4,128)(2,1)S(1)} async-done(((bf16[4,64,256]{2,0,1:T(4,128)(2,1)}), bf16[4,64,256]{2,0,1:T(4,128)(2,1)S(1)}, u32[]{:S(2)}, u32[]{:S(2)}) %all-to-all-start.2) | async-done | bytes 131104 | tf_op jit(solution)/shard_map/all_to_all | solution.py:130
  95.9 1.0 convolution_bitcast_fusion.3
  96.9 1.0 fusion.7
  98.5 14.2 %all_gather.14 = bf16[64,2048]{1,0:T(8,128)(2,1)S(1)} all-gather(bf16[8,2048]{1,0:T(8,128)(2,1)S(1)} %fusion.70), channel_id=1, replica_groups=mesh['dp'=4,'kv'=4,'tp'=2] {'kv','tp'}, dimensions={0}, use_global_device_ids=true | all-gather | bytes 294912 | tf_op jit(solution)/shard_map/all_gather | solution.py:153
  112.7 1.2 convolution_convert_fusion
  113.9 1.2 convolution_convert_fusion.1
  115.2 3.7 %all_to_all.59 = bf16[2,32,256]{2,1,0:T(8,128)(2,1)S(1)} all-to-all(bf16[2,32,256]{2,1,0:T(8,128)(2,1)S(1)} %bitcast.139), channel_id=1, replica_groups=mesh['dp'=4,'kv'=4,'tp'=2] {'tp'}, dimensions={0} | all-to-all | bytes 65536 | tf_op jit(solution)/shard_map/all_to_all | solution.py:30
  119.0 13.6 %all_gather.15 = bf16[32,2048]{1,0:T(8,128)(2,1)S(1)} all-gather(bf16[32,512]{1,0:T(8,128)(2,1)S(1)} %bitcast.141), channel_id=1, replica_groups=mesh['dp'=4,'kv'=4,'tp'=2] {'kv'}, dimensions={1}, use_global_device_ids=true | all-gather | bytes 163840 | tf_op jit(solution)/shard_map/all_gather | solution.py:32
  132.7 3.6 %convolution_multiply_fusion.1 = f32[32,1408]{1,0:T(8,128)S(1)} fusion(bf16[2048,1408]{1,0:T(8,128)(2,1)} %param.37, bf16[32,2048]{1,0:T(8,128)(2,1)S(1)} %all_gather.15, f32[2048]{0:T(1024)S(1)} %copy-done.5, f32[32]{0:T(128)S(1)} %add_rsqrt_fusion.3), kind=kOutput, calls=%fused_computation.2 | convolution fusion | flops 184791040 | bytes 6086784 | tf_op jit(solution)/shard_map/dot_general | solution.py:16
  136.3 7.0 %fusion.20 = f32[32,2048]{1,0:T(8,128)} fusion(bf16[1408,2048]{1,0:T(8,128)(2,1)} %param.39, bf16[2048,1408]{1,0:T(8,128)(2,1)} %param.38, f32[32,1408]{1,0:T(8,128)S(1)} %convolution_multiply_fusion.1, bf16[32,2048]{1,0:T(8,128)(2,1)S(1)} %all_gather.15, f32[2048]{0:T(1024)S(1)} %copy-done.5, f32[32]{0:T(128)S(1)} %add_rsqrt_fusion.3), kind=kOutput, calls=%fused_computation.40 | convolution fusion | flops 369610752 | bytes 12116096 | tf_op jit(solution)/shard_map/dot_general | solution.py:25
  143.4 2.8 %fusion.4 = f32[1,16,128,128]{3,2,1,0:T(8,128)} fusion(f32[8,16,128]{2,0,1:T(8,128)S(1)} %fusion.7, f32[1,16,128,128]{3,2,1,0:T(8,128)S(1)} %copy-done.1, f32[16]{0:T(128)S(1)} %fusion.86, f32[8,16,128]{2,1,0:T(8,128)S(1)} %get-tuple-element.24), kind=kOutput, calls=%fused_computation.9 | convolution fusion | flops 25690112 | bytes 2228288 | tf_op jit(solution)/shard_map/sthk,sthv->shkv/dot_general | solution.py:88
  146.3 16.4 %reduce-scatter.5.cloned.1.call-done = f32[32,512]{1,0:T(8,128)} async-done(((f32[32,2048]{1,0:T(8,128)}), f32[32,512]{1,0:T(8,128)}) %reduce-scatter.5.cloned.1.call-update) | async-done | bytes 65552 | tf_op jit(solution)/shard_map/reduce_scatter | solution.py:35
  163.4 3.8 %all_to_all.60 = f32[2,32,256]{2,1,0:T(8,128)S(1)} all-to-all(f32[2,32,256]{2,1,0:T(8,128)S(1)} %pad_maximum_fusion.2), channel_id=1, replica_groups=mesh['dp'=4,'kv'=4,'tp'=2] {'tp'}, dimensions={0} | all-to-all | bytes 131072 | tf_op jit(solution)/shard_map/all_to_all | solution.py:37
  (81 shorter events, 8.0 us)
Async XLA Ops:
  7.2 71.4 %copy-start = (bf16[2048,256]{1,0:T(8,128)(2,1)S(1)}, bf16[2048,256]{1,0:T(8,128)(2,1)}, u32[]{:S(2)}) copy-start(bf16[2048,256]{1,0:T(8,128)(2,1)} %param.31) | copy-start | bytes 3145732
  7.2 23.7 %copy-start.4 = (f32[2048]{0:T(1024)S(1)}, f32[2048]{0:T(1024)}, u32[]{:S(2)}) copy-start(f32[2048]{0:T(1024)} %param.23) | copy-start | bytes 24580
  7.2 52.2 %reduce-scatter.3.cloned.1.call-start = ((), (), s32[]{:S(2)}) async-start(), calls=%async_computation.7 | async-start | bytes 327680 | tf_op jit(solution)/shard_map/reduce_scatter | solution.py:35
  30.9 7.9 %copy-start.8 = (f32[16]{0:T(128)S(1)}, f32[16]{0:T(128)}, u32[]{:S(2)}) copy-start(f32[16]{0:T(128)} %param.34) | copy-start | bytes 196
  30.9 33.0 %copy-start.3 = (bf16[64,256]{1,0:T(8,128)(2,1)S(1)}, bf16[64,256]{1,0:T(8,128)(2,1)}, u32[]{:S(2)}) copy-start(bf16[64,256]{1,0:T(8,128)(2,1)} %param.20) | copy-start | bytes 98308
  30.9 47.5 %copy-start.6 = (f32[2048]{0:T(1024)S(1)}, f32[2048]{0:T(1024)}, u32[]{:S(2)}) copy-start(f32[2048]{0:T(1024)} %param.27) | copy-start | bytes 24580
  30.9 47.9 %copy-start.2 = (bf16[2048,256]{1,0:T(8,128)(2,1)S(1)}, bf16[2048,256]{1,0:T(8,128)(2,1)}, u32[]{:S(2)}) copy-start(bf16[2048,256]{1,0:T(8,128)(2,1)} %param.30) | copy-start | bytes 3145732
  38.1 48.3 %copy-start.7 = (bf16[2048,16]{0,1:T(8,128)(2,1)S(1)}, bf16[2048,16]{0,1:T(8,128)(2,1)}, u32[]{:S(2)}) copy-start(bf16[2048,16]{0,1:T(8,128)(2,1)} %param.33) | copy-start | bytes 196612
  64.0 31.9 %copy-start.1 = (f32[1,16,128,128]{3,2,1,0:T(8,128)S(1)}, f32[1,16,128,128]{3,2,1,0:T(8,128)}, u32[]{:S(2)}) copy-start(f32[1,16,128,128]{3,2,1,0:T(8,128)} %param.22) | copy-start | bytes 3145732
  80.7 52.0 %copy-start.5 = (f32[2048]{0:T(1024)S(1)}, f32[2048]{0:T(1024)}, u32[]{:S(2)}) copy-start(f32[2048]{0:T(1024)} %param.36) | copy-start | bytes 24580
  83.0 10.1 %all-to-all-start.2 = ((bf16[4,64,256]{2,0,1:T(4,128)(2,1)}), bf16[4,64,256]{2,0,1:T(4,128)(2,1)S(1)}, u32[]{:S(2)}, u32[]{:S(2)}) async-start(bf16[4,64,256]{2,0,1:T(4,128)(2,1)} %copy.88), calls=%async_computation.3 | async-start | bytes 262144 | tf_op jit(solution)/shard_map/all_to_all | solution.py:130
  86.4 76.3 %reduce-scatter.5.cloned.1.call-start = ((), (), s32[]{:S(2)}) async-start(), calls=%async_computation.8 | async-start | bytes 327680 | tf_op jit(solution)/shard_map/reduce_scatter | solution.py:35
Sparse Core Ops, SparseCore 0:
  38.2 21.0 reduce-scatter.2
  143.5 19.0 reduce-scatter.4
